TPU v7x, 512 devices: a whole 4x4x16 slice. The times are simulated.
512 devices in a mesh: sp: 128 (over z, x, core), tp: 4 (over y).
Axes of the slice: x: 4, y: 4, z: 16, core: 2. Of those that a mesh axis runs over, the one named last changes fastest.
Arguments:
- tokens: bfloat16 [16384, 2048], P('sp'), may hold values from -6 to 6
- pre_gain: float32 [2048], replicated, may hold values from 0.1 to 1.9
- outer_gate: bfloat16 [2048, 1024], P('sp', 'tp'), may hold values from -0.125 to 0.125
- inner_gate: bfloat16 [2048, 1024], P('sp', 'tp'), may hold values from -0.125 to 0.125
- conv_input: bfloat16 [2048, 1024], P('sp', 'tp'), may hold values from -0.125 to 0.125
- conv_taps: float32 [3, 1024], P(None, 'tp'), may hold values from -3.5 to 3.5
- query_down: bfloat16 [2048, 768], P(None, 'tp'), may hold values from -0.088388348 to 0.088388348
- latent_down: bfloat16 [2048, 512], P(None, 'tp'), may hold values from -0.088388348 to 0.088388348
- rotary_down: bfloat16 [2048, 32], replicated, may hold values from -0.125 to 0.125
- query_gain: float32 [768], replicated, may hold values from 1 to 3
- latent_gain: float32 [512], replicated, may hold values from 1 to 3
- query_up: bfloat16 [768, 512], P(None, 'tp'), may hold values from -0.14433757 to 0.14433757
- query_rotary: bfloat16 [768, 256], P(None, 'tp'), may hold values from -0.21875 to 0.21875
- key_up: bfloat16 [512, 512], P(None, 'tp'), may hold values from -4.33012702 to 4.33012702
- value_up: bfloat16 [512, 512], P(None, 'tp'), may hold values from -0.25 to 0.25
- conv_output: bfloat16 [1024, 2048], P('tp'), may hold values from -0.15625 to 0.15625
- heads_output: bfloat16 [512, 2048], P('tp'), may hold values from -0.15625 to 0.15625
- post_gain: float32 [2048], replicated, may hold values from 0.1 to 1.9
Outputs:
- mixed: bfloat16 [16384, 2048], P(('sp', 'tp'))
- row_logsum: float32 [8, 16384], P('tp', 'sp')
All inputs are finite; a program needn't handle non-finite values.
Results may differ from a plain program's by a relative error of at most 0.013.
Values may be sent and summed in bfloat16 or wider, within the bound.
A program may use at most 64 MiB of HBM per device.

v0:
```python
import math

import jax
import jax.numpy as jnp
from jax import lax
from jax.sharding import Mesh
from jax.sharding import PartitionSpec as P

NOPE = 64
ROPE = 32
VDIM = 64
TAPS = 3
SP = ("sp_0", "sp_1", "sp_2")
SP_TP = ("sp_0", "sp_1", "sp_2", "tp")


eps = 1e-06
rope_theta = 500000.0


def copy_for_each(array, axis):
    copies = jnp.broadcast_to(array, (lax.axis_size(axis), *array.shape))
    return lax.all_to_all(copies, axis, split_axis=0, concat_axis=0, tiled=True)


def laid_out(pieces, dim):
    shape = list(pieces.shape[1:])
    shape[dim] *= pieces.shape[0]
    return jnp.moveaxis(pieces, 0, dim).reshape(shape)


def gathered_by_axis(array, axes, dim):
    far, near = axes
    pieces = copy_for_each(copy_for_each(array, far), near)
    return laid_out(pieces.swapaxes(0, 1).reshape(-1, *array.shape), dim)


def sent_together(arrays, axis, dim, along):
    both = jnp.concatenate(arrays, axis=along)
    whole, at, done = (gathered_by_axis(both, axis, dim), 0, [])
    for a in arrays:
        done.append(lax.slice_in_dim(whole, at, at + a.shape[along], axis=along))
        at += a.shape[along]
    return tuple(done)


def shifted(value, axis, steps):
    count = lax.axis_size(axis)
    first, last = (max(0, -steps), min(count, count - steps))
    return lax.ppermute(value, axis, [(source, source + steps) for source in range(first, last)])


def one_gather(arrays, axis, dims):
    vector = jnp.concatenate([a.reshape(-1) for a in arrays])
    lines, at, done = (lax.all_gather(vector, axis), 0, [])
    for a, dim in zip(arrays, dims):
        pieces = lines[:, at : at + a.size].reshape(-1, *a.shape)
        done.append(laid_out(pieces, dim))
        at += a.size
    return tuple(done)


def side_by_side(arrays, axis, dim, along):
    both = jnp.concatenate(arrays, axis=along)
    whole, at, done = (lax.all_gather(both, axis, axis=dim, tiled=True), 0, [])
    for a in arrays:
        done.append(lax.slice_in_dim(whole, at, at + a.shape[along], axis=along))
        at += a.shape[along]
    return tuple(done)


def in_blocks(array, dim, count):
    shape = array.shape
    pieces = array.reshape(*shape[:dim], count, shape[dim] // count, *shape[dim + 1 :])
    return jnp.moveaxis(pieces, dim, 0)


def sum_at_owner(array, axis, dim):
    pieces = in_blocks(array, dim, lax.axis_size(axis))
    arrived = lax.all_to_all(pieces, axis, split_axis=0, concat_axis=0, tiled=True)
    return arrived.astype(jnp.float32).sum(axis=0)


def rms_scale(values, scale_row):
    widened = values.astype(jnp.float32)
    return (
        widened * lax.rsqrt(jnp.mean(widened * widened, axis=-1, keepdims=True) + eps) * scale_row
    )


def rotate(values, positions):
    half_width = values.shape[-1] // 2
    frequency = rope_theta ** (-jnp.arange(half_width, dtype=jnp.float32) / half_width)
    angles = positions.astype(jnp.float32)[:, None] * frequency
    cosine = jnp.cos(angles)[:, None, :]
    sine_part = jnp.sin(angles)[:, None, :]
    leading = values[..., :half_width]
    trailing = values[..., half_width:]
    return jnp.concatenate(
        [leading * cosine - trailing * sine_part, trailing * cosine + leading * sine_part], axis=-1
    )


def attend(
    state_now, query_nope, query_turned, key_nope, key_rotary, value_rows, key_first, query_position
):
    row_best, weight_sum, weighted = state_now
    heads_here = query_nope.shape[1]
    key_count = key_nope.shape[0]
    key_heads = key_nope.reshape(key_count, heads_here, NOPE)
    value_heads = value_rows.reshape(key_count, heads_here, VDIM)
    scores = jnp.einsum("qhd,khd->hqk", query_nope, key_heads, preferred_element_type=jnp.float32)
    scores = scores + jnp.einsum(
        "qhd,kd->hqk", query_turned, key_rotary, preferred_element_type=jnp.float32
    )
    scores = scores * (NOPE + ROPE) ** (-0.5)
    key_position = key_first + jnp.arange(key_count, dtype=jnp.int32)
    causal = key_position[None, :] <= query_position[:, None]
    scores = jnp.where(causal[None], scores, -1e30)
    new_best = jnp.maximum(row_best, jnp.max(scores, axis=-1))
    weights = jnp.where(causal[None], jnp.exp(scores - new_best[..., None]), 0.0)
    shrink = jnp.exp(row_best - new_best)
    weight_sum = weight_sum * shrink + jnp.sum(weights, axis=-1)
    weighted = weighted * shrink[..., None] + jnp.einsum(
        "hqk,khd->hqd",
        weights.astype(jnp.bfloat16),
        value_heads,
        preferred_element_type=jnp.float32,
    )
    return (new_best, weight_sum, weighted)


def fold_blocks(state_now, pieces, step_rule):
    total_rows = pieces[0].shape[0]
    block_width = math.gcd(total_rows, 1024)
    block_count = total_rows // block_width
    stacked = tuple(
        (member.reshape(block_count, block_width, member.shape[1]) for member in pieces)
    )

    def one_block(state_in, inputs):
        block_index, block_pieces = inputs
        return (step_rule(state_in, block_pieces, block_index * block_width), None)

    state_out, unused = lax.scan(
        one_block, state_now, (jnp.arange(block_count, dtype=jnp.int32), stacked)
    )
    return state_out


def local(
    tokens,
    pre_gain,
    outer_gate,
    inner_gate,
    conv_input,
    conv_taps,
    query_down,
    latent_down,
    rotary_down,
    query_gain,
    latent_gain,
    query_up,
    query_rotary,
    key_up,
    value_up,
    conv_output,
    heads_output,
    post_gain,
):
    row_count = tokens.shape[0]
    normed = rms_scale(tokens, pre_gain).astype(jnp.bfloat16)
    sp_index = lax.axis_index(SP)
    positions = sp_index * row_count + jnp.arange(row_count, dtype=jnp.int32)
    pieces = sent_together((outer_gate, inner_gate, conv_input), (("sp_0", "sp_1"), "sp_2"), 0, 1)
    outer_part, inner_part, signal = tuple(
        (jnp.dot(normed, member, preferred_element_type=jnp.float32) for member in pieces)
    )
    product = (inner_part * signal).astype(jnp.bfloat16)
    edge_rows = shifted(product[row_count - (TAPS - 1) :], SP, 1)
    extended = jnp.concatenate([edge_rows, product], axis=0).astype(jnp.float32)
    convolved = extended[0:row_count] * conv_taps[0]
    for offset in range(1, TAPS):
        convolved = convolved + extended[offset : offset + row_count] * conv_taps[offset]
    conv_mixed = (outer_part * convolved).astype(jnp.bfloat16)
    query_latent = jnp.dot(normed, query_down, preferred_element_type=jnp.float32).astype(
        jnp.bfloat16
    )
    key_latent = jnp.dot(normed, latent_down, preferred_element_type=jnp.float32).astype(
        jnp.bfloat16
    )
    query_latent, key_latent = one_gather((query_latent, key_latent), "tp", (1, 1))
    query_normed = rms_scale(query_latent, query_gain).astype(jnp.bfloat16)
    latent_normed = rms_scale(key_latent, latent_gain).astype(jnp.bfloat16)
    rotary_raw = jnp.dot(normed, rotary_down, preferred_element_type=jnp.float32)
    key_rotary = rotate(rotary_raw[:, None, :], positions)[:, 0, :].astype(jnp.bfloat16)
    heads_here = query_up.shape[1] // NOPE
    query_nope = jnp.dot(query_normed, query_up, preferred_element_type=jnp.float32).astype(
        jnp.bfloat16
    )
    query_nope = query_nope.reshape(row_count, heads_here, NOPE)
    turned_raw = jnp.dot(query_normed, query_rotary, preferred_element_type=jnp.float32)
    query_turned = rotate(turned_raw.reshape(row_count, heads_here, ROPE), positions).astype(
        jnp.bfloat16
    )
    key_nope = jnp.dot(latent_normed, key_up, preferred_element_type=jnp.float32).astype(
        jnp.bfloat16
    )
    value_rows = jnp.dot(latent_normed, value_up, preferred_element_type=jnp.float32).astype(
        jnp.bfloat16
    )
    initial = (
        jnp.full((heads_here, row_count), -1e30, jnp.float32),
        jnp.zeros((heads_here, row_count), jnp.float32),
        jnp.zeros((heads_here, row_count, VDIM), jnp.float32),
    )

    def heads_step(state_now, block_pieces, key_first):
        return attend(
            state_now,
            query_nope,
            query_turned,
            block_pieces[0],
            block_pieces[1],
            block_pieces[2],
            key_first,
            positions,
        )

    row_best, weight_sum, weighted = fold_blocks(
        initial, side_by_side((key_nope, key_rotary, value_rows), SP, 0, 1), heads_step
    )
    heads_mixed = (weighted / weight_sum[..., None]).astype(jnp.bfloat16)
    heads_mixed = heads_mixed.transpose(1, 0, 2).reshape(row_count, heads_here * VDIM)
    row_logsum = row_best + jnp.log(weight_sum)
    projected = sum_at_owner(
        (
            jnp.dot(conv_mixed, conv_output, preferred_element_type=jnp.float32)
            + jnp.dot(heads_mixed, heads_output, preferred_element_type=jnp.float32)
        ).astype(jnp.bfloat16),
        "tp",
        0,
    )
    mixed = rms_scale(projected, post_gain).astype(jnp.bfloat16)
    return (mixed, row_logsum)


def solution(mesh):
    split = Mesh(mesh.devices.reshape(16, 4, 2, mesh.shape["tp"]), ("sp_0", "sp_1", "sp_2", "tp"))
    return jax.shard_map(
        local,
        mesh=split,
        in_specs=(
            P(SP, None),
            P(),
            P(SP, "tp"),
            P(SP, "tp"),
            P(SP, "tp"),
            P(None, "tp"),
            P(None, "tp"),
            P(None, "tp"),
            P(),
            P(),
            P(),
            P(None, "tp"),
            P(None, "tp"),
            P(None, "tp"),
            P(None, "tp"),
            P("tp", None),
            P("tp", None),
            P(),
        ),
        out_specs=(P(SP_TP, None), P("tp", SP)),
        check_vma=False,
    )
```

profile of v0, /device:TPU:1, one launch (start us, length us, event | category | flops | bytes accessed | tf_op | source)
XLA Modules:
  0.0 311.4 jit_solution(3868678448744605362)
XLA Ops:
  7.3 1.3 fusion.22
  8.7 1.6 fusion.21
  10.3 1.8 convolution_convert_fusion
  12.4 10.8 %all-gather = bf16[163840]{0:T(1024)(128)(2,1)S(1)} all-gather(bf16[40960]{0:T(1024)(128)(2,1)S(1)} %pad_maximum_fusion), channel_id=2, replica_groups=mesh['sp_0'=16,'sp_1'=4,'sp_2'=2,'tp'=4] {'tp'}, dimensions={0}, use_global_device_ids=true | all-gather | bytes 409600 | tf_op jit(solution)/shard_map/all_gather | solution.py:55
  25.1 0.6 pad_maximum_fusion.1
  25.8 1.3 broadcast_in_dim.26
  27.0 19.1 %all-to-all-start = ((bf16[64,16,768]{2,1,0:T(8,128)(2,1)}), bf16[64,16,768]{2,1,0:T(8,128)(2,1)S(1)}, u32[]{:S(2)}, u32[]{:S(2)}) async-start(bf16[64,16,768]{2,1,0:T(8,128)(2,1)} %broadcast_in_dim.26), calls=%async_computation | async-start | bytes 3145728 | tf_op jit(solution)/shard_map/all_to_all | solution.py:23
  46.8 0.8 copy.56
  47.8 0.8 fusion.60
  48.6 0.8 multiply_cosine_fusion
  49.4 1.2 fusion.61
  50.6 0.8 fusion.31
  51.4 1.2 convolution_convert_fusion.4
  52.6 69.6 %all-to-all-done = bf16[64,16,768]{2,1,0:T(8,128)(2,1)S(1)} async-done(((bf16[64,16,768]{2,1,0:T(8,128)(2,1)}), bf16[64,16,768]{2,1,0:T(8,128)(2,1)S(1)}, u32[]{:S(2)}, u32[]{:S(2)}) %all-to-all-start) | async-done | bytes 1572896 | tf_op jit(solution)/shard_map/all_to_all | solution.py:23
  122.5 12.5 %all_to_all.15 = bf16[2,64,16,768]{3,2,1,0:T(8,128)(2,1)S(1)} all-to-all(bf16[2,64,16,768]{3,2,1,0:T(8,128)(2,1)S(1)} %broadcast_in_dim.31), channel_id=1, replica_groups=mesh['sp_0'=16,'sp_1'=4,'sp_2'=2,'tp'=4] {'sp_2'}, dimensions={0} | all-to-all | bytes 6291456 | tf_op jit(solution)/shard_map/all_to_all | solution.py:23
  135.0 0.5 copy.52
  135.4 0.6 copy-done.3
  136.4 0.7 copy-done.1
  137.5 4.4 %collective-permute-start = (bf16[2,256]{1,0:T(2,128)(2,1)S(1)}, bf16[2,256]{1,0:T(2,128)(2,1)S(1)}, u32[]{:S(2)}, u32[]{:S(2)}) collective-permute-start(bf16[2,256]{1,0:T(2,128)(2,1)S(1)} %slice.79), channel_id=1, source_target_pairs={{0,4},{4,8},{8,12},{12,16},{16,20},{20,24},{24,28},{28,32},{32,36}... | collective-permute-start | bytes 3080 | tf_op jit(solution)/shard_map/ppermute | solution.py:50
  141.9 0.7 collective-permute-done
  142.6 2.0 fusion.20
  144.6 70.6 %all-gather.3.cloned.1.call-done = bf16[16384,288]{0,1:T(8,128)(2,1)} async-done(((bf16[128,288]{0,1:T(8,128)(2,1)}), bf16[16384,288]{0,1:T(8,128)(2,1)}) %all-gather.3.cloned.1.call-update) | async-done | bytes 9437200 | tf_op jit(solution)/shard_map/all_gather | solution.py:65
  215.2 1.3 slice.88
  216.6 3.9 %fusion.59 = (bf16[16384,128]{0,1:T(8,128)(2,1)S(1)}, bf16[16384,128]{0,1:T(8,128)(2,1)S(1)}) fusion(bf16[16384,288]{0,1:T(8,128)(2,1)} %all-gather.3.cloned.1.call-done), kind=kLoop, calls=%fused_computation.109 | loop fusion | bytes 16777216 | tf_op jit(solution)/shard_map/slice | solution.py:67
  220.5 4.3 %copy_bitcast_fusion = (bf16[16,1024,128]{1,2,0:T(8,128)(2,1)}, bf16[16,1024,128]{1,2,0:T(8,128)(2,1)}) fusion(bf16[16,16,8,1024]{3,2,1,0:T(8,128)(2,1)S(1)} %bitcast.114, bf16[16,16,8,1024]{3,2,1,0:T(8,128)(2,1)S(1)} %bitcast.115), kind=kLoop, calls=%fused_computation.28 | loop fusion | bytes 16777216
  224.8 63.5 %while.15 = (s32[]{:T(128)}, f32[2,128]{1,0:T(2,128)S(1)}, f32[2,128]{1,0:T(2,128)S(1)}, f32[2,128,64]{1,2,0:T(8,128)S(1)}, s32[16]{0:T(128)S(1)}, /*index=5*/bf...) while((s32[]{:T(128)}, f32[2,128]{1,0:T(2,128)S(1)}, ...), condition=%wide.region_7.8_spmd.clone, body=%wide.region_4.7_spmd.clone.sunk | while | flops 86690176 | bytes 7611585 | solution.py:145
  224.8 0.6 dynamic_slice.32
  226.3 1.1 constant_dynamic-slice_fusion.3
  228.8 0.6 dynamic_slice.32
  230.2 1.1 constant_dynamic-slice_fusion.3
  232.7 0.6 dynamic_slice.32
  234.2 1.1 constant_dynamic-slice_fusion.3
  235.6 0.4 fusion.94
  236.7 0.6 dynamic_slice.32
  238.2 1.1 constant_dynamic-slice_fusion.3
  240.7 0.6 dynamic_slice.32
  242.2 1.1 constant_dynamic-slice_fusion.3
  244.6 0.6 dynamic_slice.32
  246.1 1.1 constant_dynamic-slice_fusion.3
  248.6 0.6 dynamic_slice.32
  250.1 1.1 constant_dynamic-slice_fusion.3
  252.6 0.6 dynamic_slice.32
  254.1 1.1 constant_dynamic-slice_fusion.3
  256.6 0.6 dynamic_slice.32
  258.0 1.1 constant_dynamic-slice_fusion.3
  260.5 0.6 dynamic_slice.32
  262.0 1.1 constant_dynamic-slice_fusion.3
  264.5 0.6 dynamic_slice.32
  266.0 1.1 constant_dynamic-slice_fusion.3
  268.5 0.6 dynamic_slice.32
  269.9 1.1 constant_dynamic-slice_fusion.3
  272.4 0.6 dynamic_slice.32
  273.9 1.1 constant_dynamic-slice_fusion.3
  276.4 0.6 dynamic_slice.32
  277.9 1.1 constant_dynamic-slice_fusion.3
  280.4 0.6 dynamic_slice.32
  281.8 1.1 constant_dynamic-slice_fusion.3
  284.3 0.6 dynamic_slice.32
  285.8 1.1 constant_dynamic-slice_fusion.3
  288.3 2.2 fusion.17
  290.5 4.0 %all-to-all-start.2 = ((bf16[4,32,2048]{2,1,0:T(8,128)(2,1)}), bf16[4,32,2048]{2,1,0:T(8,128)(2,1)S(1)}, u32[]{:S(2)}, u32[]{:S(2)}) async-start(bf16[4,32,2048]{2,1,0:T(8,128)(2,1)} %bitcast.22), calls=%async_computation.2 | async-start | bytes 1048576 | tf_op jit(solution)/shard_map/all_to_all | solution.py:80
  294.5 0.6 log_add_fusion
  295.1 8.5 %all-to-all-done.2 = bf16[4,32,2048]{2,1,0:T(8,128)(2,1)S(1)} async-done(((bf16[4,32,2048]{2,1,0:T(8,128)(2,1)}), bf16[4,32,2048]{2,1,0:T(8,128)(2,1)S(1)}, u32[]{:S(2)}, u32[]{:S(2)}) %all-to-all-start.2) | async-done | bytes 524320 | tf_op jit(solution)/shard_map/all_to_all | solution.py:80
  303.8 0.8 multiply_convert_fusion.1
  (240 shorter events, 29.2 us)
Async XLA Ops:
  7.2 135.4 %copy-start = (bf16[256,2048]{1,0:T(8,128)(2,1)S(1)}, bf16[256,2048]{1,0:T(8,128)(2,1)}, u32[]{:S(2)}) copy-start(bf16[256,2048]{1,0:T(8,128)(2,1)} %param.35) | copy-start | bytes 3145732
  7.2 16.4 %copy-start.2 = (bf16[128,2048]{1,0:T(8,128)(2,1)S(1)}, bf16[128,2048]{1,0:T(8,128)(2,1)}, u32[]{:S(2)}) copy-start(bf16[128,2048]{1,0:T(8,128)(2,1)} %param.20) | copy-start | bytes 1572868
  7.2 16.4 %copy-start.7 = (f32[2048]{0:T(1024)S(1)}, f32[2048]{0:T(1024)}, u32[]{:S(2)}) copy-start(f32[2048]{0:T(1024)} %param.21) | copy-start | bytes 24580
  7.2 16.4 %copy-start.18 = (bf16[2048,32]{0,1:T(8,128)(2,1)S(1)}, bf16[2048,32]{0,1:T(8,128)(2,1)}, u32[]{:S(2)}) copy-start(bf16[2048,32]{0,1:T(8,128)(2,1)} %param.28) | copy-start | bytes 393220
  7.2 17.0 %copy-start.12 = (f32[512]{0:T(512)S(1)}, f32[512]{0:T(512)}, u32[]{:S(2)}) copy-start(f32[512]{0:T(512)} %param.30) | copy-start | bytes 6148
  7.2 17.2 %copy-start.4 = (bf16[512,128]{1,0:T(8,128)(2,1)S(1)}, bf16[512,128]{1,0:T(8,128)(2,1)}, u32[]{:S(2)}) copy-start(bf16[512,128]{1,0:T(8,128)(2,1)} %param.34) | copy-start | bytes 393220
  7.2 208.0 %all-gather.3.cloned.1.call-start = ((), (), s32[]{:S(2)}) async-start(), calls=%async_computation.3 | async-start | bytes 9510912 | tf_op jit(solution)/shard_map/all_gather | solution.py:65
  7.3 17.6 %copy-start.13 = (f32[16]{0:T(128)}, f32[16]{0:T(128)S(1)}, u32[]{:S(2)}) copy-start(f32[16]{0:T(128)S(1)} %multiply_power_fusion) | copy-start | bytes 196
  7.3 17.4 %copy-start.5 = (bf16[512,128]{1,0:T(8,128)(2,1)S(1)}, bf16[512,128]{1,0:T(8,128)(2,1)}, u32[]{:S(2)}) copy-start(bf16[512,128]{1,0:T(8,128)(2,1)} %param.33) | copy-start | bytes 393220
  8.7 16.0 %copy-start.16 = (f32[128]{0:T(128)}, f32[128]{0:T(128)S(1)}, u32[]{:S(2)}) copy-start(f32[128]{0:T(128)S(1)} %add_rsqrt_fusion.3) | copy-start | bytes 1540
  8.7 17.0 %copy-start.9 = (bf16[16,256]{1,0:T(8,128)(2,1)S(1)}, bf16[16,256]{1,0:T(8,128)(2,1)}, u32[]{:S(2)}) copy-start(bf16[16,256]{1,0:T(8,128)(2,1)} %param.24) | copy-start | bytes 24580
  8.7 17.0 %copy-start.10 = (bf16[16,256]{1,0:T(8,128)(2,1)S(1)}, bf16[16,256]{1,0:T(8,128)(2,1)}, u32[]{:S(2)}) copy-start(bf16[16,256]{1,0:T(8,128)(2,1)} %param.23) | copy-start | bytes 24580
  8.7 17.0 %copy-start.11 = (bf16[16,256]{1,0:T(8,128)(2,1)S(1)}, bf16[16,256]{1,0:T(8,128)(2,1)}, u32[]{:S(2)}) copy-start(bf16[16,256]{1,0:T(8,128)(2,1)} %param.22) | copy-start | bytes 24580
  23.5 22.6 %copy-start.6 = (f32[768]{0:T(1024)S(1)}, f32[768]{0:T(1024)}, u32[]{:S(2)}) copy-start(f32[768]{0:T(1024)} %param.29) | copy-start | bytes 9220
  23.6 3.4 %copy-start.14 = (f32[128]{0:T(128)}, f32[128]{0:T(128)S(1)}, u32[]{:S(2)}) copy-start(f32[128]{0:T(128)S(1)} %add_convert_fusion.1) | copy-start | bytes 1540
  27.0 95.2 %all-to-all-start = ((bf16[64,16,768]{2,1,0:T(8,128)(2,1)}), bf16[64,16,768]{2,1,0:T(8,128)(2,1)S(1)}, u32[]{:S(2)}, u32[]{:S(2)}) async-start(bf16[64,16,768]{2,1,0:T(8,128)(2,1)} %broadcast_in_dim.26), calls=%async_computation | async-start | bytes 3145728 | tf_op jit(solution)/shard_map/all_to_all | solution.py:23
  46.7 0.9 copy-start.15
  135.0 1.0 copy-start.3
  135.0 1.0 copy-start.17
  135.4 1.7 copy-start.1
  137.5 5.1 %collective-permute-start = (bf16[2,256]{1,0:T(2,128)(2,1)S(1)}, bf16[2,256]{1,0:T(2,128)(2,1)S(1)}, u32[]{:S(2)}, u32[]{:S(2)}) collective-permute-start(bf16[2,256]{1,0:T(2,128)(2,1)S(1)} %slice.79), channel_id=1, source_target_pairs={{0,4},{4,8},{8,12},{12,16},{16,20},{20,24},{24,28},{28,32},{32,36}... | collective-permute-start | bytes 3080 | tf_op jit(solution)/shard_map/ppermute | solution.py:50
  288.3 15.5 %copy-start.8 = (f32[2048]{0:T(1024)S(1)}, f32[2048]{0:T(1024)}, u32[]{:S(2)}) copy-start(f32[2048]{0:T(1024)} %param.37) | copy-start | bytes 24580
  290.5 13.1 %all-to-all-start.2 = ((bf16[4,32,2048]{2,1,0:T(8,128)(2,1)}), bf16[4,32,2048]{2,1,0:T(8,128)(2,1)S(1)}, u32[]{:S(2)}, u32[]{:S(2)}) async-start(bf16[4,32,2048]{2,1,0:T(8,128)(2,1)} %bitcast.22), calls=%async_computation.2 | async-start | bytes 1048576 | tf_op jit(solution)/shard_map/all_to_all | solution.py:80
Sparse Core Ops, SparseCore 0:
  25.8 189.3 all-gather.2
where the time goes:
time: 312 us; the launch traced here: 311 us
  waiting for transfers between devices  149 us (48%)
  local copies, waits for them, and re-layouts  42.1 us (13%)
  matrix products  29.3 us (9%)
  starting transfers between devices  27.5 us (9%)
  blocking collectives  23.3 us (7%)
  between operations  14.6 us (5%)
  other arithmetic  13.5 us (4%)
  loops' own time  11.6 us (4%)
    all_gather x1, waiting for transfers between devices, side_by_side(): whole, at, done = (lax.all_gather(both, axis, axis=dim, tiled=True), 0, [])  70.6 us
    all_to_all x1, waiting for transfers between devices, copy_for_each(): return lax.all_to_all(copies, axis, split_axis=0, concat_axis=0, tiled=True)  69.6 us
    dynamic_slice x32, local copies, waits for them, and re-layouts, fold_blocks(): lax.scan(one_block, state_now, (jnp.arange(block_count, dtype=jnp.int32),...  26.5 us
    all_to_all x1, starting transfers between devices, copy_for_each(): return lax.all_to_all(copies, axis, split_axis=0, concat_axis=0, tiled=True)  19.1 us
    all_to_all x1, blocking collectives, copy_for_each(): return lax.all_to_all(copies, axis, split_axis=0, concat_axis=0, tiled=True)  12.5 us
    another operation x1, loops' own time, fold_blocks(): lax.scan(one_block, state_now, (jnp.arange(block_count, dtype=jnp.int32),...  11.6 us
    all_gather x1, blocking collectives, one_gather(): lines, at, done = (lax.all_gather(vector, axis), 0, [])  10.8 us
    all_to_all x1, waiting for transfers between devices, sum_at_owner(): lax.all_to_all(pieces, axis, split_axis=0, concat_axis=0, tiled=True)  8.47 us
  transfers between devices with their start and end apart: 4, of which 4 were waited for; matrix products, arithmetic and copies ran while one was open for 4% of the time, Pallas kernels for 0%

commit v1 on v0

v1 whole, which is shorter than its diff:
```python
import math

import jax
import jax.numpy as jnp
import numpy as np
from jax import lax
from jax.experimental import pallas as pl
from jax.experimental.pallas import tpu as pltpu
from jax.sharding import Mesh
from jax.sharding import PartitionSpec as P

NOPE = 64
ROPE = 32
VDIM = 64
EPS = 1e-06
THETA = 500000.0
NZ, NX, NC, NY = 16, 4, 2, 4
NP = NX * NC
ROWS = 128
HEADS = 2
SLAB = NP * ROWS
UP, DOWN = NZ // 2, NZ // 2 - 1
PIECES = 3
PIECE = 96
KV_ROWS = 288
TILE = 256
AHEAD = 3
LOG2E = math.log2(math.e)
SCALE2 = (NOPE + ROPE) ** (-0.5) * LOG2E
LOW = -1e30
F32 = jnp.float32
BF16 = jnp.bfloat16
MESH = pl.DeviceIdType.MESH
SP = ("z", "x", "c")


def angle_tables():
    half = ROPE // 2
    frequency = THETA ** (-np.arange(half, dtype=np.float64) / half)
    near = np.arange(ROWS, dtype=np.float64)
    far = np.arange(NZ * NP, dtype=np.float64) * ROWS
    parts = []
    for places in (near, far):
        angles = frequency[:, None] * places[None, :]
        parts += [np.cos(angles), np.sin(angles)]
    return np.concatenate(parts, axis=0).astype(np.float32)


def dot(a, b):
    return jnp.dot(a, b, preferred_element_type=F32)


def kernel(
    tokens, pre_gain, outer_gate, inner_gate, conv_input, taps, query_down, latent_down,
    rotary_down, query_gain, latent_gain, query_up, query_rotary, key_up, value_up,
    conv_output, heads_output, post_gain, angles,
    out, logsum,
    normed, weights, latk, latq, kv, queries, blocks, acc, stats, sent_o, sent_s, got_o, got_s,
    product, sums, got_sums,
    w_got, w_sib_got, w_sent_z, w_sent_x, w_sent_f, w_sib_sent,
    kv_got, kv_sent, k_got, k_sent, q_got, q_sent, g_got, g_sent,
    o_got, o_sent, s_got, s_sent, h_got, h_sent, y_got, y_sent,
):
    z, x, c, y = (lax.axis_index(a) for a in ("z", "x", "c", "y"))
    me = x * NC + c
    zup, zdown = lax.rem(z + 1, NZ), lax.rem(z + NZ - 1, NZ)
    xright, xleft = lax.rem(x + 1, NX), lax.rem(x + NX - 1, NX)
    xfar = lax.rem(x + 2, NX)
    has_next = jnp.logical_or(me < NP - 1, z < NZ - 1)
    has_prev = jnp.logical_or(me > 0, z > 0)
    next_p = lax.rem(me + 1, NP)
    next_dev = {
        "z": jnp.minimum(z + jnp.where(me == NP - 1, 1, 0), NZ - 1),
        "x": next_p // NC,
        "c": lax.rem(next_p, NC),
    }
    prev_dev = {
        "z": jnp.maximum(z - 1, 0),
        "x": NX - 1,
        "c": NC - 1,
    }

    def slab_dev(p):
        return {"x": p // NC, "c": lax.rem(p, NC)}

    def remote(src, dst, ssem, rsem, dev):
        return pltpu.make_async_remote_copy(
            src_ref=src, dst_ref=dst, send_sem=ssem, recv_sem=rsem, device_id=dev, device_id_type=MESH
        )

    weights[z, x, c, :, 0:256] = outer_gate[...]
    weights[z, x, c, :, 256:512] = inner_gate[...]
    weights[z, x, c, :, 512:768] = conv_input[...]

    barrier = pltpu.get_barrier_semaphore()

    def greet(dev):
        pl.semaphore_signal(barrier, inc=1, device_id=dev, device_id_type=MESH)

    greet({"z": zup})
    greet({"z": zdown})
    for d in range(1, NP):
        greet(slab_dev(lax.rem(me + d, NP)))
    for d in range(1, NY):
        greet({"y": lax.rem(y + d, NY)})
    far_next = jnp.logical_and(me == NP - 1, z < NZ - 1)
    far_prev = jnp.logical_and(me == 0, z > 0)

    @pl.when(far_next)
    def _():
        greet(next_dev)

    @pl.when(far_prev)
    def _():
        greet(prev_dev)

    pl.semaphore_wait(
        barrier, 2 + NP - 1 + NY - 1 + jnp.where(far_next, 1, 0) + jnp.where(far_prev, 1, 0)
    )

    def up_origin(s):
        return lax.rem(z + NZ - s, NZ)

    def down_origin(s):
        return lax.rem(z + s, NZ)

    def w_copy(origin, column, ssem, dev):
        block = weights.at[origin, column, c]
        return remote(block, block, ssem, w_got.at[column, origin], dev)

    def w_z(way, s):
        origin = up_origin(s) if way == 0 else down_origin(s)
        return w_copy(origin, x, w_sent_z.at[way, s], {"z": zup if way == 0 else zdown})

    def w_x(way, origin):
        return w_copy(origin, x, w_sent_x.at[way, origin], {"x": xright if way == 0 else xleft})

    def w_forward(way, origin):
        column, dev = (xleft, xright) if way == 0 else (xright, xleft)
        return w_copy(origin, column, w_sent_f.at[origin], {"x": dev})

    def w_sibling(origin):
        half = weights.at[origin, :, c]
        return remote(half, half, w_sib_sent.at[origin], w_sib_got.at[origin], {"c": 1 - c})

    def w_wait(column, origin):
        w_copy(origin, column, w_sent_f.at[origin], {"x": xright}).wait_recv()

    def w_start():
        w_z(0, 0).start()
        w_z(1, 0).start()
        w_x(0, z).start()
        w_x(1, z).start()

    def w_step_z(s):
        for way, last in ((0, UP), (1, DOWN)):
            origin = up_origin(s) if way == 0 else down_origin(s)

            @pl.when(s <= last)
            def _():
                w_wait(x, origin)

                @pl.when(s < last)
                def _():
                    w_z(way, s).start()

                w_x(0, origin).start()
                w_x(1, origin).start()

    def w_each(s, act):
        act(up_origin(s))

        @pl.when(jnp.logical_and(s >= 1, s <= DOWN))
        def _():
            act(down_origin(s))

    def w_step_x(s):
        def act(origin):
            w_wait(xleft, origin)
            w_wait(xright, origin)
            even = lax.rem(origin, 2) == 0

            @pl.when(even)
            def _():
                w_forward(0, origin).start()

            @pl.when(jnp.logical_not(even))
            def _():
                w_forward(1, origin).start()

        w_each(s, act)

    def w_step_sibling(s):
        def act(origin):
            w_wait(xfar, origin)
            w_sibling(origin).start()

        w_each(s, act)

    w_start()

    wide = tokens[...].astype(F32)
    scaled = wide * lax.rsqrt(jnp.mean(wide * wide, axis=-1, keepdims=True) + EPS) * pre_gain[...]
    normed[...] = scaled.astype(BF16)

    latk[y] = dot(normed[...], latent_down[...]).astype(BF16)

    def k_copy(d):
        return remote(latk.at[y], latk.at[y], k_sent.at[d], k_got.at[y], {"y": lax.rem(y + d, NY)})

    def k_arrival(d):
        other = lax.rem(y + d, NY)
        return remote(latk.at[other], latk.at[other], k_sent.at[d], k_got.at[other], {"y": other})

    def q_copy(d):
        return remote(latq.at[y], latq.at[y], q_sent.at[d], q_got.at[y], {"y": lax.rem(y + d, NY)})

    def q_arrival(d):
        other = lax.rem(y + d, NY)
        return remote(latq.at[other], latq.at[other], q_sent.at[d], q_got.at[other], {"y": other})

    for d in range(1, NY):
        k_copy(d).start()
    latq[y] = dot(normed[...], query_down[...]).astype(BF16)
    for d in range(1, NY):
        q_copy(d).start()

    lane = lax.broadcasted_iota(jnp.int32, (ROPE // 2, ROWS), 1)
    mine = lane == z * NP + me

    def far_value(rows):
        return jnp.sum(jnp.where(mine, rows, 0.0), axis=1, keepdims=True)

    cos_near, sin_near = angles[0:16, :], angles[16:32, :]
    cos_far, sin_far = far_value(angles[32:48, :]), far_value(angles[48:64, :])
    cosine = cos_near * cos_far - sin_near * sin_far
    sine = sin_near * cos_far + cos_near * sin_far

    def rotated(turned):
        lead, trail = turned[0:16, :], turned[16:32, :]
        return jnp.concatenate([lead * cosine - trail * sine, trail * cosine + lead * sine], axis=0)

    key_rotary = rotated(dot(normed[...], rotary_down[...]).T).astype(BF16)
    w_step_z(jnp.int32(1))

    for d in range(1, NY):
        k_arrival(d).wait_recv()
    latent = jnp.concatenate([latk[i] for i in range(NY)], axis=1).astype(F32)
    latent = latent * lax.rsqrt(jnp.mean(latent * latent, axis=-1, keepdims=True) + EPS)
    latent = (latent * latent_gain[...]).astype(BF16)
    kv[z, 0:128, :] = dot(latent, key_up[...]).astype(BF16)
    kv[z, 128:256, :] = dot(latent, value_up[...]).T.astype(BF16)
    kv[z, 256:288, :] = key_rotary

    def kv_copy(way, s, piece):
        origin = up_origin(s) if way == 0 else down_origin(s)
        rows = kv.at[origin, pl.ds(pl.multiple_of(piece * PIECE, PIECE), PIECE)]
        return remote(
            rows, rows, kv_sent.at[way, s, piece], kv_got.at[origin, piece],
            {"z": zup if way == 0 else zdown},
        )

    def kv_sends(way, s):
        if way == 0:
            return jnp.logical_and(s < UP, jnp.logical_and(z - s >= 0, z < NZ - 1))
        return jnp.logical_and(s < DOWN, down_origin(s) < DOWN)

    def kv_comes(way, s):
        if way == 0:
            return z - s >= 0
        return jnp.logical_and(s <= DOWN, down_origin(s) < DOWN)

    for way in range(2):

        @pl.when(kv_sends(way, 0))
        def _():
            for piece in range(PIECES):
                kv_copy(way, 0, piece).start()

    for d in range(1, NY):
        q_arrival(d).wait_recv()
    parts = [latq[i].astype(F32) for i in range(NY)]
    square = sum(jnp.sum(p * p, axis=-1, keepdims=True) for p in parts)
    factor = lax.rsqrt(square * (1.0 / (NY * parts[0].shape[1])) + EPS)
    nope, turned = None, None
    for i in range(NY):
        part = (parts[i] * factor * query_gain[i : i + 1, :]).astype(BF16)
        rows = slice(i * part.shape[1], (i + 1) * part.shape[1])
        a, b = dot(part, query_up[rows, :]), dot(part, query_rotary[rows, :])
        nope = a if nope is None else nope + a
        turned = b if turned is None else turned + b
    turned = turned.T
    queries[me, 0:128, :] = nope.T.astype(BF16)
    queries[me, 128:160, :] = rotated(turned[0:32, :]).astype(BF16)
    queries[me, 160:192, :] = rotated(turned[32:64, :]).astype(BF16)

    def g_copy(d):
        return remote(
            queries.at[me], queries.at[me], g_sent.at[d], g_got.at[me], slab_dev(lax.rem(me + d, NP))
        )

    def g_arrival(d):
        other = lax.rem(me + d, NP)
        return remote(queries.at[other], queries.at[other], g_sent.at[d], g_got.at[other], slab_dev(other))

    for d in range(1, NP):
        g_copy(d).start()

    w_step_x(jnp.int32(0))
    w_step_z(jnp.int32(2))
    w_step_x(jnp.int32(1))
    w_step_sibling(jnp.int32(0))
    w_step_z(jnp.int32(3))

    acc[...] = jnp.zeros_like(acc)
    stats[0:HEADS, :] = jnp.full((HEADS, SLAB), LOW, F32)
    stats[HEADS : 2 * HEADS, :] = jnp.zeros((HEADS, SLAB), F32)
    for d in range(1, NP):
        g_arrival(d).wait_recv()
    blocks[...] = jnp.zeros_like(blocks)
    for p in range(NP):
        for h in range(HEADS):
            columns = slice(h * SLAB + p * ROWS, h * SLAB + (p + 1) * ROWS)
            blocks[h * NOPE : (h + 1) * NOPE, columns] = queries[p, h * NOPE : (h + 1) * NOPE, :]
            blocks[128:160, columns] = queries[p, 128 + h * ROPE : 128 + (h + 1) * ROPE, :]

    def attend(origin, diagonal):
        keys = kv[origin, 0:128, :]
        rotary = kv[origin, 256:288, :].astype(F32).T.astype(BF16)
        keys = jnp.concatenate([keys, rotary], axis=1)
        for h in range(HEADS):
            values = kv[origin, 128 + h * VDIM : 128 + (h + 1) * VDIM, :]
            for t in range(SLAB // TILE):
                at = slice(t * TILE, (t + 1) * TILE)
                scores = dot(keys, blocks[:, h * SLAB + t * TILE : h * SLAB + (t + 1) * TILE]) * SCALE2
                if diagonal:
                    key = me * ROWS + lax.broadcasted_iota(jnp.int32, (ROWS, TILE), 0)
                    query = t * TILE + lax.broadcasted_iota(jnp.int32, (ROWS, TILE), 1)
                    seen = key <= query
                    scores = jnp.where(seen, scores, LOW)
                old = stats[h : h + 1, at]
                best = jnp.maximum(old, jnp.max(scores, axis=0, keepdims=True))
                weight = jnp.exp2(scores - best)
                if diagonal:
                    weight = jnp.where(seen, weight, 0.0)
                shrink = jnp.exp2(old - best)
                stats[h : h + 1, at] = best
                total = slice(HEADS + h, HEADS + h + 1)
                stats[total, at] = stats[total, at] * shrink + jnp.sum(weight, axis=0, keepdims=True)
                acc[h, :, at] = acc[h, :, at] * shrink + dot(values, weight.astype(BF16))

    attend(z, True)

    def ring_step(s, carry):
        for piece in range(PIECES):
            for way in range(2):

                @pl.when(kv_comes(way, s))
                def _():
                    origin = up_origin(s) if way == 0 else down_origin(s)
                    rows = kv.at[origin, pl.ds(piece * PIECE, PIECE)]
                    remote(
                        rows, rows, kv_sent.at[way, 0, piece], kv_got.at[origin, piece], {"z": zup}
                    ).wait_recv()

                    @pl.when(kv_sends(way, s))
                    def _():
                        kv_copy(way, s, piece).start()

        w_step_z(s + AHEAD)

        @pl.when(s + 1 <= UP)
        def _():
            w_step_x(s + 1)

        w_step_sibling(s)

        @pl.when(z - s >= 0)
        def _():
            attend(up_origin(s), False)

        @pl.when(jnp.logical_and(s <= DOWN, z + s >= NZ))
        def _():
            attend(down_origin(s), False)

        return carry

    lax.fori_loop(1, UP + 1, ring_step, jnp.int32(0))

    for p in range(NP):
        at = slice(p * ROWS, (p + 1) * ROWS)
        for h in range(HEADS):
            sent_o[p, h * VDIM : (h + 1) * VDIM, :] = acc[h, :, at].astype(BF16)
        sent_s[p, 0 : 2 * HEADS, :] = stats[:, at]
        sent_s[p, 2 * HEADS : 8, :] = jnp.zeros((8 - 2 * HEADS, ROWS), F32)

    def o_copy(d):
        p = lax.rem(me + d, NP)
        return remote(sent_o.at[p], got_o.at[me], o_sent.at[d], o_got.at[me], slab_dev(p))

    def s_copy(d):
        p = lax.rem(me + d, NP)
        return remote(sent_s.at[p], got_s.at[me], s_sent.at[d], s_got.at[me], slab_dev(p))

    def o_arrival(d):
        p = lax.rem(me + d, NP)
        return remote(sent_o.at[p], got_o.at[p], o_sent.at[d], o_got.at[p], slab_dev(p))

    def s_arrival(d):
        p = lax.rem(me + d, NP)
        return remote(sent_s.at[p], got_s.at[p], s_sent.at[d], s_got.at[p], slab_dev(p))

    for d in range(1, NP):
        o_copy(d).start()
        s_copy(d).start()
    got_o[me] = sent_o[me]
    got_s[me] = sent_s[me]

    mixed_in = None
    for k in range(NZ // 2):
        for i in range(2):
            half = weights.at[2 * k + i, :, 1 - c]
            remote(
                half, half, w_sib_sent.at[2 * k + i], w_sib_got.at[2 * k + i], {"c": 1 - c}
            ).wait_recv()
        part = dot(
            normed[:, 256 * k : 256 * (k + 1)],
            weights[2 * k : 2 * k + 2].reshape(256, 768),
        )
        mixed_in = part if mixed_in is None else mixed_in + part
    outer_part = mixed_in[:, 0:256]
    product[16:144, :] = (mixed_in[:, 256:512] * mixed_in[:, 512:768]).astype(BF16)

    h_copy = remote(product.at[pl.ds(128, 16)], product.at[pl.ds(0, 16)], h_sent, h_got, next_dev)

    @pl.when(has_next)
    def _():
        h_copy.start()

    @pl.when(has_prev)
    def _():
        h_copy.wait_recv()

    @pl.when(jnp.logical_not(has_prev))
    def _():
        product[0:16, :] = jnp.zeros((16, 256), BF16)

    extended = product[...].astype(F32)
    convolved = pltpu.roll(extended, 2, axis=0)[16:144] * taps[0:1, :]
    convolved = convolved + pltpu.roll(extended, 1, axis=0)[16:144] * taps[1:2, :]
    convolved = convolved + extended[16:144] * taps[2:3, :]
    conv_mixed = (outer_part * convolved).astype(BF16)

    for d in range(1, NP):
        o_arrival(d).wait_recv()
        s_arrival(d).wait_recv()
    heads = []
    for h in range(HEADS):
        best = got_s[0, h : h + 1, :]
        for p in range(1, NP):
            best = jnp.maximum(best, got_s[p, h : h + 1, :])
        total, weighted = None, None
        for p in range(NP):
            factor = jnp.exp2(got_s[p, h : h + 1, :] - best)
            a = got_s[p, HEADS + h : HEADS + h + 1, :] * factor
            b = got_o[p, h * VDIM : (h + 1) * VDIM, :].astype(F32) * factor
            total = a if total is None else total + a
            weighted = b if weighted is None else weighted + b
        logsum[h : h + 1, :] = (best + jnp.log2(total)) * (1.0 / LOG2E)
        heads.append(weighted / total)
    heads_mixed = jnp.concatenate(heads, axis=0).T.astype(BF16)

    quarter = ROWS // NY

    def y_copy(d):
        p = lax.rem(y + d, NY)
        return remote(sums.at[p], got_sums.at[y], y_sent.at[d], y_got.at[y], {"y": p})

    def y_arrival(d):
        p = lax.rem(y + d, NY)
        return remote(sums.at[p], got_sums.at[p], y_sent.at[d], y_got.at[p], {"y": p})

    for t in range(4):
        at = slice(t * 512, (t + 1) * 512)
        projected = dot(conv_mixed, conv_output[:, at]) + dot(heads_mixed, heads_output[:, at])
        for p in range(NY):
            sums[p, :, at] = projected[p * quarter : (p + 1) * quarter, :].astype(BF16)
    for d in range(1, NY):
        y_copy(d).start()
    whole = sums[y].astype(F32)
    for d in range(1, NY):
        y_arrival(d).wait_recv()
        whole = whole + got_sums[lax.rem(y + d, NY)].astype(F32)
    whole = whole * lax.rsqrt(jnp.mean(whole * whole, axis=-1, keepdims=True) + EPS) * post_gain[...]
    out[...] = whole.astype(BF16)

    for d in range(1, NY):
        k_copy(d).wait_send()
        q_copy(d).wait_send()
        y_copy(d).wait_send()
    for d in range(1, NP):
        g_copy(d).wait_send()
        o_copy(d).wait_send()
        s_copy(d).wait_send()

    @pl.when(has_next)
    def _():
        h_copy.wait_send()

    def left(s, carry):
        @pl.when(s < UP)
        def _():
            w_z(0, s).wait_send()

        @pl.when(s < DOWN)
        def _():
            w_z(1, s).wait_send()

        w_x(0, s).wait_send()
        w_x(1, s).wait_send()
        w_forward(0, s).wait_send()
        w_sibling(s).wait_send()
        for way in range(2):

            @pl.when(kv_sends(way, s))
            def _():
                for piece in range(PIECES):
                    kv_copy(way, s, piece).wait_send()

        return carry

    lax.fori_loop(0, NZ, left, jnp.int32(0))


def local(
    tokens, pre_gain, outer_gate, inner_gate, conv_input, conv_taps, query_down, latent_down,
    rotary_down, query_gain, latent_gain, query_up, query_rotary, key_up, value_up,
    conv_output, heads_output, post_gain,
):
    width = tokens.shape[1]
    vmem = pl.BlockSpec(memory_space=pltpu.VMEM)
    dma = pltpu.SemaphoreType.DMA
    scratch = [
        pltpu.VMEM((ROWS, width), BF16),
        pltpu.VMEM((NZ, NX, NC, 16, 768), BF16),
        pltpu.VMEM((NY, ROWS, 128), BF16),
        pltpu.VMEM((NY, ROWS, 192), BF16),
        pltpu.VMEM((NZ, KV_ROWS, ROWS), BF16),
        pltpu.VMEM((NP, 192, ROWS), BF16),
        pltpu.VMEM((160, HEADS * SLAB), BF16),
        pltpu.VMEM((HEADS, VDIM, SLAB), F32),
        pltpu.VMEM((2 * HEADS, SLAB), F32),
        pltpu.VMEM((NP, HEADS * VDIM, ROWS), BF16),
        pltpu.VMEM((NP, 8, ROWS), F32),
        pltpu.VMEM((NP, HEADS * VDIM, ROWS), BF16),
        pltpu.VMEM((NP, 8, ROWS), F32),
        pltpu.VMEM((16 + ROWS, 256), BF16),
        pltpu.VMEM((NY, ROWS // NY, width), BF16),
        pltpu.VMEM((NY, ROWS // NY, width), BF16),
        dma((NX, NZ)),
        dma((NZ,)),
        dma((2, UP)),
        dma((2, NZ)),
        dma((NZ,)),
        dma((NZ,)),
        dma((NZ, PIECES)),
        dma((2, UP, PIECES)),
        dma((NY,)),
        dma((NY,)),
        dma((NY,)),
        dma((NY,)),
        dma((NP,)),
        dma((NP,)),
        dma((NP,)),
        dma((NP,)),
        dma((NP,)),
        dma((NP,)),
        dma,
        dma,
        dma((NY,)),
        dma((NY,)),
    ]
    return pl.pallas_call(
        kernel,
        out_shape=(
            jax.ShapeDtypeStruct((ROWS // NY, width), BF16),
            jax.ShapeDtypeStruct((HEADS, ROWS), F32),
        ),
        in_specs=[vmem] * 19,
        out_specs=(vmem, vmem),
        scratch_shapes=scratch,
        compiler_params=pltpu.CompilerParams(
            collective_id=0, has_side_effects=True, vmem_limit_bytes=48 * 1024 * 1024
        ),
        name="layer",
    )(
        tokens, pre_gain.reshape(1, -1), outer_gate, inner_gate, conv_input, conv_taps, query_down,
        latent_down, rotary_down, query_gain.reshape(NY, -1), latent_gain.reshape(1, -1), query_up,
        query_rotary, key_up, value_up, conv_output, heads_output, post_gain.reshape(1, -1),
        jnp.asarray(angle_tables()),
    )


def solution(mesh):
    split = Mesh(mesh.devices.reshape(NZ, NX, NC, NY), ("z", "x", "c", "y"))
    return jax.shard_map(
        local,
        mesh=split,
        in_specs=(
            P(SP, None), P(), P(SP, "y"), P(SP, "y"), P(SP, "y"), P(None, "y"), P(None, "y"),
            P(None, "y"), P(), P(), P(), P(None, "y"), P(None, "y"), P(None, "y"), P(None, "y"),
            P("y", None), P("y", None), P(),
        ),
        out_specs=(P(("z", "x", "c", "y"), None), P("y", SP)),
        check_vma=False,
    )
```

time: 312 us -> 83.9 us (0.27)
  waiting for transfers between devices: 149 us -> 0 us
  Pallas kernels: 0 us -> 69.4 us
  matrix products: 29.3 us -> 0 us
  local copies, waits for them, and re-layouts: 42.1 us -> 13.1 us
  starting transfers between devices: 27.5 us -> 0 us
  blocking collectives: 23.3 us -> 0 us
  between operations: 14.6 us -> 0.77 us
  other arithmetic: 13.5 us -> 0 us
  loops' own time: 11.6 us -> 0 us
    all_to_all x2 -> x0, waiting for transfers between devices: 78.1 us -> none  [the longest x1 69.6 us: copy_for_each(): return lax.all_to_all(copies, axis, split_axis=0, concat_axis=0, tiled=True)]
    all_gather x1 -> x0, waiting for transfers between devices: 70.6 us -> none  [side_by_side(): whole, at, done = (lax.all_gather(both, axis, axis=dim, tiled=True), 0, [])]
    pallas_call x0 -> x1, Pallas kernels: none -> 69.4 us  [local(): pl.pallas_call(kernel, out_shape=(jax.ShapeDtypeStruct((ROWS // NY, width...]
    dot_general x59 -> x0, matrix products: 29.3 us -> none  [the longest x16 6.24 us: attend(): jnp.einsum('qhd,kd->hqk', query_turned, key_rotary, preferred_element_typ...]
    dynamic_slice x32 -> x0, local copies, waits for them, and re-layouts: 26.5 us -> none  [fold_blocks(): lax.scan(one_block, state_now, (jnp.arange(block_count, dtype=jnp.int32),...]
    all_to_all x2 -> x0, starting transfers between devices: 23.1 us -> none  [the longest x1 19.1 us: copy_for_each(): return lax.all_to_all(copies, axis, split_axis=0, concat_axis=0, tiled=True)]
    all_to_all x1 -> x0, blocking collectives: 12.5 us -> none  [copy_for_each(): return lax.all_to_all(copies, axis, split_axis=0, concat_axis=0, tiled=True)]
    another operation x1 -> x0, loops' own time: 11.6 us -> none  [fold_blocks(): lax.scan(one_block, state_now, (jnp.arange(block_count, dtype=jnp.int32),...]
  transfers between devices with their start and end apart: 4 -> 0, of which waited for: 4 -> 0; matrix products, arithmetic and copies ran while one was open for 4% -> 0% of each run, Pallas kernels for 0% -> 0%
where the time goes in v1:
time: 83.9 us; the launch traced here: 83.3 us
  Pallas kernels  69.4 us (83%)
  local copies, waits for them, and re-layouts  13.1 us (16%)
    pallas_call x1, Pallas kernels, local(): pl.pallas_call(kernel, out_shape=(jax.ShapeDtypeStruct((ROWS // NY, width...  69.4 us
    unnamed x39, local copies, waits for them, and re-layouts  13 us

profile of v1, /device:TPU:1, one launch (start us, length us, event | category | flops | bytes accessed | tf_op | source)
XLA Modules:
  0.0 83.3 jit_solution(17391153286287532773)
XLA Ops:
  0.6 0.0 copy-start.16
  0.6 0.7 copy-done.16
  1.3 0.1 reshape.17.query_gain
  1.4 0.0 copy-start.15
  1.4 1.1 %copy.23.query_rotary = bf16[768,64]{1,0:T(8,128)(2,1)S(1)} copy(bf16[768,64]{0,1:T(8,128)(2,1)} %param.31) | data formatting | bytes 196608 | tf_op args[12]
  2.5 0.0 copy-done.15
  2.5 0.3 copy.22.rotary_down
  2.8 0.0 copy-start
  2.8 0.0 copy-start.1
  2.8 0.0 copy-start.4
  2.8 0.0 copy-start.8
  2.9 0.0 copy-start.13
  2.9 1.6 %copy.21.query_down = bf16[2048,192]{1,0:T(8,128)(2,1)S(1)} copy(bf16[2048,192]{0,1:T(8,128)(2,1)} %param.25) | data formatting | bytes 1572864 | tf_op args[6]
  4.4 0.0 copy-done
  4.4 0.0 copy-done.1
  4.5 0.0 copy-done.4
  4.5 0.0 copy-done.8
  4.5 0.0 copy-done.13
  4.5 0.0 copy-start.2
  4.5 1.0 %copy-done.2 = bf16[2048,128]{1,0:T(8,128)(2,1)S(1)} copy-done((bf16[2048,128]{1,0:T(8,128)(2,1)S(1)}, bf16[2048,128]{1,0:T(8,128)(2,1)}, u32[]{:S(2)}) %copy-start.2) | copy-done | bytes 524312
  5.5 0.0 copy-start.3
  5.5 1.0 %copy-done.3 = bf16[128,2048]{1,0:T(8,128)(2,1)S(1)} copy-done((bf16[128,2048]{1,0:T(8,128)(2,1)S(1)}, bf16[128,2048]{1,0:T(8,128)(2,1)}, u32[]{:S(2)}) %copy-start.3) | copy-done | bytes 524312
  6.6 0.0 copy-start.5
  6.6 0.9 %copy-done.5 = bf16[512,128]{1,0:T(8,128)(2,1)S(1)} copy-done((bf16[512,128]{1,0:T(8,128)(2,1)S(1)}, bf16[512,128]{1,0:T(8,128)(2,1)}, u32[]{:S(2)}) %copy-start.5) | copy-done | bytes 131096
  7.5 0.0 copy-start.6
  7.5 0.9 %copy-done.6 = bf16[512,128]{1,0:T(8,128)(2,1)S(1)} copy-done((bf16[512,128]{1,0:T(8,128)(2,1)S(1)}, bf16[512,128]{1,0:T(8,128)(2,1)}, u32[]{:S(2)}) %copy-start.6) | copy-done | bytes 131096
  8.4 0.0 copy-start.7
  8.4 0.8 copy-done.7
  9.1 0.0 copy-start.9
  9.1 0.7 copy-done.9
  9.8 0.0 copy-start.10
  9.8 0.7 copy-done.10
  10.5 0.0 copy-start.11
  10.5 0.7 copy-done.11
  11.2 0.0 copy-start.12
  11.2 0.7 copy-done.12
  11.9 0.0 copy-start.14
  11.9 0.7 copy-done.14
  12.6 69.4 %layer.1 = (bf16[32,2048]{1,0:T(8,128)(2,1)S(1)}, f32[2,128]{1,0:T(2,128)S(1)}) custom-call(bf16[128,2048]{1,0:T(8,128)(2,1)S(1)} %copy-done.1, f32[1,2048]{1,0:T(1,128)S(1)} %bitcast.3, bf16[16,256]{1,0:T(8,128)(2,1)S(1)} %copy-done.9, bf16[16,256]{1,0:T(8,128)(2,1)S(1)} %copy-done.10, bf16[16,256]{1,0:T(8,128)(2,1)S(1)} %copy-done.11, ...), custom_call_target="tpu_custom_call" | custom-call | tf_op jit(solution)/shard_map/layer/pallas_call | solution.py:583
  82.1 0.7 copy.26
  82.7 0.6 copy.27
Async XLA Ops:
  0.6 0.7 copy-start.16
  1.4 1.1 %copy-start.15 = (bf16[2048,32]{0,1:T(8,128)(2,1)S(1)}, bf16[2048,32]{0,1:T(8,128)(2,1)}, u32[]{:S(2)}) copy-start(bf16[2048,32]{0,1:T(8,128)(2,1)} %param.27) | copy-start | bytes 393220
  2.8 1.6 %copy-start = (bf16[256,2048]{1,0:T(8,128)(2,1)S(1)}, bf16[256,2048]{1,0:T(8,128)(2,1)}, u32[]{:S(2)}) copy-start(bf16[256,2048]{1,0:T(8,128)(2,1)} %conv_output.1) | copy-start | bytes 3145732
  2.8 1.6 %copy-start.1 = (bf16[128,2048]{1,0:T(8,128)(2,1)S(1)}, bf16[128,2048]{1,0:T(8,128)(2,1)}, u32[]{:S(2)}) copy-start(bf16[128,2048]{1,0:T(8,128)(2,1)} %tokens.1) | copy-start | bytes 1572868
  2.8 1.6 %copy-start.4 = (bf16[768,128]{1,0:T(8,128)(2,1)S(1)}, bf16[768,128]{1,0:T(8,128)(2,1)}, u32[]{:S(2)}) copy-start(bf16[768,128]{1,0:T(8,128)(2,1)} %query_up.1) | copy-start | bytes 589828
  2.8 1.6 %copy-start.8 = (f32[2048]{0:T(1024)S(1)}, f32[2048]{0:T(1024)}, u32[]{:S(2)}) copy-start(f32[2048]{0:T(1024)} %param.20) | copy-start | bytes 24580
  2.9 1.6 %copy-start.13 = (f32[3,256]{1,0:T(4,128)S(1)}, f32[3,256]{1,0:T(4,128)}, u32[]{:S(2)}) copy-start(f32[3,256]{1,0:T(4,128)} %taps.1) | copy-start | bytes 9220
  4.5 1.0 %copy-start.2 = (bf16[2048,128]{1,0:T(8,128)(2,1)S(1)}, bf16[2048,128]{1,0:T(8,128)(2,1)}, u32[]{:S(2)}) copy-start(bf16[2048,128]{1,0:T(8,128)(2,1)} %latent_down.1) | copy-start | bytes 1572868
  5.5 1.0 %copy-start.3 = (bf16[128,2048]{1,0:T(8,128)(2,1)S(1)}, bf16[128,2048]{1,0:T(8,128)(2,1)}, u32[]{:S(2)}) copy-start(bf16[128,2048]{1,0:T(8,128)(2,1)} %heads_output.1) | copy-start | bytes 1572868
  6.6 0.9 %copy-start.5 = (bf16[512,128]{1,0:T(8,128)(2,1)S(1)}, bf16[512,128]{1,0:T(8,128)(2,1)}, u32[]{:S(2)}) copy-start(bf16[512,128]{1,0:T(8,128)(2,1)} %key_up.1) | copy-start | bytes 393220
  7.5 0.9 %copy-start.6 = (bf16[512,128]{1,0:T(8,128)(2,1)S(1)}, bf16[512,128]{1,0:T(8,128)(2,1)}, u32[]{:S(2)}) copy-start(bf16[512,128]{1,0:T(8,128)(2,1)} %value_up.1) | copy-start | bytes 393220
  8.4 0.8 copy-start.7
  9.1 0.7 copy-start.9
  9.8 0.7 copy-start.10
  10.5 0.7 copy-start.11
  11.2 0.7 copy-start.12
  11.9 0.7 copy-start.14

commit v2 on v1

--- a/solution.py
+++ b/solution.py
@@ -51,10 +51,12 @@
 
 
 def kernel(
-    tokens, pre_gain, outer_gate, inner_gate, conv_input, taps, query_down, latent_down,
-    rotary_down, query_gain, latent_gain, query_up, query_rotary, key_up, value_up,
-    conv_output, heads_output, post_gain, angles,
+    tokens_h, pre_gain_h, outer_gate_h, inner_gate_h, conv_input_h, taps_h, query_down_h, latent_down_h,
+    rotary_down_h, query_gain_h, latent_gain_h, query_up_h, query_rotary_h, key_up_h, value_up_h,
+    conv_output_h, heads_output_h, post_gain_h, angles_h,
     out, logsum,
+    tokens, pre_gain, taps, down, latent_down, query_gain, latent_gain, query_up, query_rotary,
+    key_up, value_up, conv_output, heads_output, post_gain, angles, up_turned, gain_turned, loaded,
     normed, weights, latk, latq, kv, queries, blocks, acc, stats, sent_o, sent_s, got_o, got_s,
     product, sums, got_sums,
     w_got, w_sib_got, w_sent_z, w_sent_x, w_sent_f, w_sib_sent,
@@ -88,9 +90,33 @@
             src_ref=src, dst_ref=dst, send_sem=ssem, recv_sem=rsem, device_id=dev, device_id_type=MESH
         )
 
-    weights[z, x, c, :, 0:256] = outer_gate[...]
-    weights[z, x, c, :, 256:512] = inner_gate[...]
-    weights[z, x, c, :, 512:768] = conv_input[...]
+    own = weights.at[z, x, c]
+    loads = [
+        pltpu.make_async_copy(src, dst, loaded.at[i])
+        for i, (src, dst) in enumerate((
+            (outer_gate_h, own.at[:, 0:256]),
+            (inner_gate_h, own.at[:, 256:512]),
+            (conv_input_h, own.at[:, 512:768]),
+            (tokens_h, tokens),
+            (pre_gain_h, pre_gain),
+            (latent_down_h, latent_down),
+            (query_down_h, down.at[0:192]),
+            (rotary_down_h, down.at[192:224]),
+            (angles_h, angles),
+            (query_up_h, query_up),
+            (latent_gain_h, latent_gain),
+            (key_up_h, key_up),
+            (value_up_h, value_up),
+            (query_gain_h, query_gain),
+            (query_rotary_h, query_rotary),
+            (taps_h, taps),
+            (conv_output_h, conv_output),
+            (heads_output_h, heads_output),
+            (post_gain_h, post_gain),
+        ))
+    ]
+    for load in loads:
+        load.start()
 
     barrier = pltpu.get_barrier_semaphore()
 
@@ -197,8 +223,12 @@
 
         w_each(s, act)
 
+    for load in loads[0:3]:
+        load.wait()
     w_start()
 
+    for load in loads[3:6]:
+        load.wait()
     wide = tokens[...].astype(F32)
     scaled = wide * lax.rsqrt(jnp.mean(wide * wide, axis=-1, keepdims=True) + EPS) * pre_gain[...]
     normed[...] = scaled.astype(BF16)
@@ -221,7 +251,12 @@
 
     for d in range(1, NY):
         k_copy(d).start()
-    latq[y] = dot(normed[...], query_down[...]).astype(BF16)
+    for load in loads[6:10]:
+        load.wait()
+    lowered = lax.dot_general(
+        down[...], normed[...], (((1,), (1,)), ((), ())), preferred_element_type=F32
+    )
+    latq[y] = lowered[0:192, :].astype(BF16)
     for d in range(1, NY):
         q_copy(d).start()
 
@@ -240,11 +275,16 @@
         lead, trail = turned[0:16, :], turned[16:32, :]
         return jnp.concatenate([lead * cosine - trail * sine, trail * cosine + lead * sine], axis=0)
 
-    key_rotary = rotated(dot(normed[...], rotary_down[...]).T).astype(BF16)
+    key_rotary = rotated(lowered[192:224, :]).astype(BF16)
+    up_turned[...] = query_up[...].astype(F32).T.astype(BF16)
+    for load in loads[10:15]:
+        load.wait()
+    gain_turned[...] = jnp.broadcast_to(query_gain[...], (ROWS, 768)).T
     w_step_z(jnp.int32(1))
 
     for d in range(1, NY):
         k_arrival(d).wait_recv()
+
     latent = jnp.concatenate([latk[i] for i in range(NY)], axis=1).astype(F32)
     latent = latent * lax.rsqrt(jnp.mean(latent * latent, axis=-1, keepdims=True) + EPS)
     latent = (latent * latent_gain[...]).astype(BF16)
@@ -279,18 +319,14 @@
 
     for d in range(1, NY):
         q_arrival(d).wait_recv()
+
     parts = [latq[i].astype(F32) for i in range(NY)]
-    square = sum(jnp.sum(p * p, axis=-1, keepdims=True) for p in parts)
-    factor = lax.rsqrt(square * (1.0 / (NY * parts[0].shape[1])) + EPS)
-    nope, turned = None, None
-    for i in range(NY):
-        part = (parts[i] * factor * query_gain[i : i + 1, :]).astype(BF16)
-        rows = slice(i * part.shape[1], (i + 1) * part.shape[1])
-        a, b = dot(part, query_up[rows, :]), dot(part, query_rotary[rows, :])
-        nope = a if nope is None else nope + a
-        turned = b if turned is None else turned + b
-    turned = turned.T
-    queries[me, 0:128, :] = nope.T.astype(BF16)
+    square = sum(jnp.sum(p * p, axis=0, keepdims=True) for p in parts)
+    factor = lax.rsqrt(square * (1.0 / (NY * parts[0].shape[0])) + EPS)
+    latent_q = jnp.concatenate(parts, axis=0) * factor * gain_turned[...]
+    latent_q = latent_q.astype(BF16)
+    queries[me, 0:128, :] = dot(up_turned[...], latent_q).astype(BF16)
+    turned = dot(query_rotary[...], latent_q)
     queries[me, 128:160, :] = rotated(turned[0:32, :]).astype(BF16)
     queries[me, 160:192, :] = rotated(turned[32:64, :]).astype(BF16)
 
@@ -351,6 +387,7 @@
 
     attend(z, True)
 
+
     def ring_step(s, carry):
         for piece in range(PIECES):
             for way in range(2):
@@ -416,6 +453,8 @@
     got_o[me] = sent_o[me]
     got_s[me] = sent_s[me]
 
+    for load in loads[15:19]:
+        load.wait()
     mixed_in = None
     for k in range(NZ // 2):
         for i in range(2):
@@ -454,6 +493,7 @@
     for d in range(1, NP):
         o_arrival(d).wait_recv()
         s_arrival(d).wait_recv()
+
     heads = []
     for h in range(HEADS):
         best = got_s[0, h : h + 1, :]
@@ -542,9 +582,27 @@
     dma = pltpu.SemaphoreType.DMA
     scratch = [
         pltpu.VMEM((ROWS, width), BF16),
+        pltpu.VMEM((1, width), F32),
+        pltpu.VMEM((3, 256), F32),
+        pltpu.VMEM((224, width), BF16),
+        pltpu.VMEM((width, 128), BF16),
+        pltpu.VMEM((1, 768), F32),
+        pltpu.VMEM((1, 512), F32),
+        pltpu.VMEM((768, 128), BF16),
+        pltpu.VMEM((64, 768), BF16),
+        pltpu.VMEM((512, 128), BF16),
+        pltpu.VMEM((512, 128), BF16),
+        pltpu.VMEM((256, width), BF16),
+        pltpu.VMEM((128, width), BF16),
+        pltpu.VMEM((1, width), F32),
+        pltpu.VMEM((64, 128), F32),
+        pltpu.VMEM((128, 768), BF16),
+        pltpu.VMEM((768, 128), F32),
+        dma((19,)),
+        pltpu.VMEM((ROWS, width), BF16),
         pltpu.VMEM((NZ, NX, NC, 16, 768), BF16),
         pltpu.VMEM((NY, ROWS, 128), BF16),
-        pltpu.VMEM((NY, ROWS, 192), BF16),
+        pltpu.VMEM((NY, 192, ROWS), BF16),
         pltpu.VMEM((NZ, KV_ROWS, ROWS), BF16),
         pltpu.VMEM((NP, 192, ROWS), BF16),
         pltpu.VMEM((160, HEADS * SLAB), BF16),
@@ -586,17 +644,17 @@
             jax.ShapeDtypeStruct((ROWS // NY, width), BF16),
             jax.ShapeDtypeStruct((HEADS, ROWS), F32),
         ),
-        in_specs=[vmem] * 19,
+        in_specs=[pl.BlockSpec(memory_space=pltpu.HBM)] * 19,
         out_specs=(vmem, vmem),
         scratch_shapes=scratch,
         compiler_params=pltpu.CompilerParams(
-            collective_id=0, has_side_effects=True, vmem_limit_bytes=48 * 1024 * 1024
+            collective_id=0, has_side_effects=True, vmem_limit_bytes=67043328
         ),
         name="layer",
     )(
-        tokens, pre_gain.reshape(1, -1), outer_gate, inner_gate, conv_input, conv_taps, query_down,
-        latent_down, rotary_down, query_gain.reshape(NY, -1), latent_gain.reshape(1, -1), query_up,
-        query_rotary, key_up, value_up, conv_output, heads_output, post_gain.reshape(1, -1),
+        tokens, pre_gain.reshape(1, -1), outer_gate, inner_gate, conv_input, conv_taps, query_down.T,
+        latent_down, rotary_down.T, query_gain.reshape(1, -1), latent_gain.reshape(1, -1), query_up,
+        query_rotary.T, key_up, value_up, conv_output, heads_output, post_gain.reshape(1, -1),
         jnp.asarray(angle_tables()),
     )
 

time: 83.9 us -> 74.2 us (0.88)
  local copies, waits for them, and re-layouts: 13.1 us -> 3.39 us
    unnamed x39 -> x6, local copies, waits for them, and re-layouts: 13 us -> 2.81 us
where the time goes in v2:
time: 74.2 us; the launch traced here: 74.1 us
  Pallas kernels  70 us (94%)
  local copies, waits for them, and re-layouts  3.39 us (5%)
    pallas_call x1, Pallas kernels, local(): pl.pallas_call(kernel, out_shape=(jax.ShapeDtypeStruct((ROWS // NY, width...  70 us
    unnamed x6, local copies, waits for them, and re-layouts  2.81 us

profile of v2, /device:TPU:1, one launch (start us, length us, event | category | flops | bytes accessed | tf_op | source)
XLA Modules:
  0.0 74.1 jit_solution(18205264267500661819)
XLA Ops:
  0.6 0.0 copy-start
  0.6 0.7 copy-done
  1.3 0.6 reshape.17.query_gain_h
  1.9 70.0 %layer.1 = (bf16[32,2048]{1,0:T(8,128)(2,1)}, f32[2,128]{1,0:T(2,128)}) custom-call(bf16[128,2048]{1,0:T(8,128)(2,1)} %tokens_h.1, f32[1,2048]{1,0:T(1,128)} %bitcast.9, bf16[16,256]{1,0:T(8,128)(2,1)} %outer_gate_h.1, bf16[16,256]{1,0:T(8,128)(2,1)} %inner_gate_h.1, bf16[16,256]{1,0:T(8,128)(2,1)} %conv_input_h.1, f32[3,256]{1,0:T(4,128)} %taps_h.1, ...), custom_call_target="tpu_custom_call" | custom-call | tf_op jit(solution)/shard_map/layer/pallas_call | solution.py:641
  71.9 0.0 copy-start.1
  71.9 1.6 %copy.23 = bf16[32,2048]{1,0:T(8,128)(2,1)} copy(bf16[32,2048]{1,0:T(8,128)(2,1)} %get-tuple-element.4) | data formatting | bytes 262144
  73.5 0.0 copy-done.1
  73.5 0.6 copy.24
Async XLA Ops:
  0.6 0.7 copy-start
  71.9 1.6 %copy-start.1 = (f32[2,128]{1,0:T(2,128)S(1)}, f32[2,128]{1,0:T(2,128)}, u32[]{:S(2)}) copy-start(f32[2,128]{1,0:T(2,128)} %get-tuple-element.5) | copy-start | bytes 3076
